TPU v7x, 32 devices: a whole 2x2x4 slice. The times are simulated.
32 devices in a mesh: sp: 16 (over z, y, x), tp: 2 (over core).
Axes of the slice: x: 2, y: 2, z: 4, core: 2. Of those that a mesh axis runs over, the one named last changes fastest.
Arguments:
- queries: bfloat16 [4096, 1024], P('sp', 'tp'), may hold values from -100 to 100
- keys: bfloat16 [256, 4096], P('tp', 'sp'), may hold values from -5 to 5
- values: bfloat16 [256, 4096], P('tp', 'sp'), may hold values from -4.5 to 4.5
- gate_cache: float32 [8, 4096], P('tp', 'sp'), as said below
- documents: int32 [4096], P('sp'), may hold values from 0 to 2, never falling along the last dimension, each value on 1 to 2560 neighbouring positions
- residual: bfloat16 [4096, 2048], P(('sp', 'tp')), may hold values from -3 to 3
- out_weight: bfloat16 [1024, 2048], replicated, may hold values from -2 to 2
- mix_gain: bfloat16 [2048], replicated, may hold values from 0.099609375 to 1.8984375
- routes: int32 [4096, 4], P(('sp', 'tp')), may hold values from 0 to 31, all different within a row; in each aligned block of 128 rows (0 to 127, 128 to 255, ...) at most 32 rows name the same one
- route_weight: float32 [4096, 4], P(('sp', 'tp')), may hold values from 0.25 to 1
- expert_gate: bfloat16 [32, 2048, 512], P(('sp', 'tp')), may hold values from -0.125 to 0.125
- expert_up: bfloat16 [32, 2048, 512], P(('sp', 'tp')), may hold values from -0.125 to 0.125
- expert_down: bfloat16 [32, 512, 2048], P(('sp', 'tp')), may hold values from -0.25 to 0.25
- shared_gate: bfloat16 [2048, 512], replicated, may hold values from -0.125 to 0.125
- shared_up: bfloat16 [2048, 512], replicated, may hold values from -0.125 to 0.125
- shared_down: bfloat16 [512, 2048], replicated, may hold values from -0.25 to 0.25
- ffn_gain: bfloat16 [2048], replicated, may hold values from 0.099609375 to 1.8984375
Outputs:
- result: bfloat16 [4096, 2048], P(('sp', 'tp'))
Inputs may be any that keep to these rules, and one draw needn't show every extreme that they name: `gate_cache`: entry (h, j) is the sum of head h's log forget gates over positions 0 to j. `documents`: never falls along the positions; no document has more than 2560 positions. `routes`: each row names 4 different experts; in the rows of one device (aligned blocks of 128 rows) no expert is named more than 32 times, a bound that some block reaches.
All inputs are finite; a program needn't handle non-finite values.
Results may differ from a plain program's by a relative error of at most 0.013.
Values may be sent and summed in bfloat16 or wider, within the bound.
A program may use at most 256 MiB of HBM per device.

v0:
```python
import jax
import jax.numpy as jnp
from jax import lax
from jax.sharding import PartitionSpec as P

HD = 128
residual_scale = 2.0**0.25
norm_epsilon = 1e-05
masked_score = -1e30


def normalize(summed, gain_vector):
    row_mean = jnp.mean(summed, axis=-1, keepdims=True)
    centred = summed - row_mean
    spread = jnp.mean(centred * centred, axis=-1, keepdims=True)
    return (centred * lax.rsqrt(spread + norm_epsilon) * gain_vector.astype(jnp.float32)).astype(
        jnp.bfloat16
    )


def expert_block(arrived, expert_gate, expert_up, expert_down):
    own_count = expert_gate.shape[0]
    grouped = arrived.reshape(-1, own_count, arrived.shape[1], arrived.shape[2])
    gate_part = jnp.einsum(
        "nemd,edf->nemf", grouped, expert_gate, preferred_element_type=jnp.float32
    )
    up_part = jnp.einsum("nemd,edf->nemf", grouped, expert_up, preferred_element_type=jnp.float32)
    hidden = (jax.nn.silu(gate_part) * up_part).astype(jnp.bfloat16)
    produced = jnp.einsum("nemf,efd->nemd", hidden, expert_down, preferred_element_type=jnp.float32)
    return produced.astype(jnp.bfloat16).reshape(arrived.shape)


def local(
    queries,
    keys,
    values,
    gate_cache,
    documents,
    residual,
    out_weight,
    mix_gain,
    routes,
    route_weight,
    expert_gate,
    expert_up,
    expert_down,
    shared_gate,
    shared_up,
    shared_down,
    ffn_gain,
):
    tok_rows = queries.shape[0]
    local_heads = gate_cache.shape[0]
    kv_local = keys.shape[0] // HD
    group_size = local_heads // kv_local
    score_scale = HD ** (-0.5)
    seq_start = lax.axis_index("sp") * tok_rows
    query_pos = seq_start + jnp.arange(tok_rows, dtype=jnp.int32)
    query_last = seq_start + tok_rows - 1
    query_cum = jnp.transpose(gate_cache).reshape(tok_rows, kv_local, group_size)
    grouped_q = queries.reshape(tok_rows, kv_local, group_size, HD)
    all_cache, all_docs = (
        lax.all_gather(gate_cache, "sp", axis=1, tiled=True),
        lax.all_gather(documents.reshape(1, tok_rows), "sp", axis=1, tiled=True),
    )
    doc_line = all_docs[0]
    initial = (
        jnp.full((tok_rows, kv_local, group_size), masked_score, jnp.float32),
        jnp.zeros((tok_rows, kv_local, group_size), jnp.float32),
        jnp.zeros((tok_rows, kv_local, group_size, HD), jnp.float32),
    )
    key_piece = lax.all_gather(keys, "sp", axis=1, tiled=True)
    value_piece = lax.all_gather(values, "sp", axis=1, tiled=True)
    width_keys = key_piece.shape[1]
    key_cum = all_cache.reshape(kv_local, group_size, width_keys)

    def update(state):
        running_max, running_sum, numerator = state
        key_block = key_piece.reshape(kv_local, HD, width_keys)
        value_block = value_piece.reshape(kv_local, HD, width_keys)
        scores = (
            jnp.einsum("qagd,adk->qagk", grouped_q, key_block, preferred_element_type=jnp.float32)
            * score_scale
        )
        scores = scores + query_cum[..., None] - key_cum[None]
        key_pos = jnp.arange(width_keys, dtype=jnp.int32)
        allowed = (key_pos[None, :] <= query_pos[:, None]) & (
            doc_line[None, :] == documents[:, None]
        )
        allowed = allowed[:, None, None, :]
        scores = jnp.where(allowed, scores, masked_score)
        new_max = jnp.maximum(running_max, jnp.max(scores, axis=-1))
        weights = jnp.where(allowed, jnp.exp(scores - new_max[..., None]), 0.0)
        new_sum = jnp.sum(weights, axis=-1)
        added = jnp.einsum(
            "qagk,adk->qagd",
            weights.astype(jnp.bfloat16),
            value_block,
            preferred_element_type=jnp.float32,
        )
        return (new_max, new_sum, added)

    active = (jnp.int32(0) <= query_last) & (doc_line[width_keys - 1] >= documents[0])
    running_max, running_sum, numerator = lax.cond(active, update, lambda state: state, initial)
    attended = (
        (numerator / running_sum[..., None])
        .astype(jnp.bfloat16)
        .reshape(tok_rows, local_heads * HD)
    )
    token_heads = lax.all_to_all(attended, "tp", split_axis=0, concat_axis=1, tiled=True)
    mixed = jnp.dot(token_heads, out_weight, preferred_element_type=jnp.float32)
    mixed = lax.optimization_barrier(mixed.astype(jnp.bfloat16)).astype(jnp.float32)
    settled = normalize(residual_scale * residual.astype(jnp.float32) + mixed, mix_gain)
    row_count = settled.shape[0]
    width_model = settled.shape[1]
    top_count = routes.shape[1]
    expert_total = lax.axis_size(("sp", "tp")) * expert_gate.shape[0]
    capacity = row_count * lax.axis_size("tp") * top_count // expert_total
    chosen_experts = routes.reshape(-1)
    matches = (
        chosen_experts[:, None] == jnp.arange(expert_total, dtype=jnp.int32)[None, :]
    ).astype(jnp.int32)
    ranks = jnp.sum(jnp.cumsum(matches, axis=0) * matches, axis=1) - 1
    slots = chosen_experts * capacity + ranks
    placing = slots[None, :] == jnp.arange(expert_total * capacity, dtype=jnp.int32)[:, None]
    placing = jnp.any(
        placing.reshape(expert_total * capacity, row_count, top_count), axis=2
    ).astype(jnp.bfloat16)
    outgoing = jnp.dot(placing, settled, preferred_element_type=jnp.float32).astype(jnp.bfloat16)
    outgoing = outgoing.reshape(expert_total, capacity, width_model)
    finished = expert_block(
        lax.all_to_all(outgoing, ("sp", "tp"), split_axis=0, concat_axis=0, tiled=True),
        expert_gate,
        expert_up,
        expert_down,
    )
    returned = lax.all_to_all(finished, ("sp", "tp"), split_axis=0, concat_axis=0, tiled=True)
    returned = returned.reshape(expert_total * capacity, width_model)
    picked_rows = jnp.take(returned, slots, axis=0).reshape(row_count, top_count, width_model)
    routed = jnp.einsum("rkd,rk->rd", picked_rows.astype(jnp.float32), route_weight)
    shared_gate_part = jnp.dot(settled, shared_gate, preferred_element_type=jnp.float32)
    shared_up_part = jnp.dot(settled, shared_up, preferred_element_type=jnp.float32)
    shared_hidden = (jax.nn.silu(shared_gate_part) * shared_up_part).astype(jnp.bfloat16)
    shared = jnp.dot(shared_hidden, shared_down, preferred_element_type=jnp.float32)
    return normalize(residual_scale * settled.astype(jnp.float32) + routed + shared, ffn_gain)


def solution(mesh):
    placed = (
        P("sp", "tp"),
        P("tp", "sp"),
        P("tp", "sp"),
        P("tp", "sp"),
        P("sp"),
        P(("sp", "tp"), None),
        P(),
        P(),
        P(("sp", "tp"), None),
        P(("sp", "tp"), None),
        P(("sp", "tp"), None, None),
        P(("sp", "tp"), None, None),
        P(("sp", "tp"), None, None),
        P(),
        P(),
        P(),
        P(),
    )
    return jax.shard_map(
        local, mesh=mesh, in_specs=placed, out_specs=P(("sp", "tp"), None), check_vma=False
    )
```

profile of v0, /device:TPU:0, one launch (start us, length us, event | category | flops | bytes accessed | tf_op | source)
XLA Modules:
  0.0 393.6 jit_solution(2535516395564024456)
XLA Ops:
  6.5 1.7 copy.56
  10.1 1.2 slice.14
  11.3 42.7 %all-gather.1 = s32[16,1,256]{2,1,0:T(1,128)S(1)} all-gather(s32[1,1,256]{2,1,0:T(1,128)} %bitcast.172), channel_id=2, replica_groups=mesh['sp'=16,'tp'=2] {'sp'}, dimensions={0}, use_global_device_ids=true | all-gather | bytes 17408 | tf_op jit(solution)/shard_map/all_gather | solution.py:64
  58.3 36.1 %all_gather.14 = f32[4,4096]{1,0:T(4,128)S(1)} all-gather(f32[4,256]{1,0:T(4,128)} %param.22), channel_id=1, replica_groups=mesh['sp'=16,'tp'=2] {'sp'}, dimensions={1}, use_global_device_ids=true | all-gather | bytes 69632 | tf_op jit(solution)/shard_map/all_gather | solution.py:63
  95.4 29.3 %all-gather.7.cloned.1.call-done = bf16[128,4096]{1,0:T(8,128)(2,1)} async-done(((bf16[128,256]{1,0:T(8,128)(2,1)}), bf16[128,4096]{1,0:T(8,128)(2,1)}) %all-gather.7.cloned.1.call-update) | async-done | bytes 1048592 | tf_op jit(solution)/shard_map/all_gather | solution.py:73
  124.7 20.7 %conditional.1 = (f32[256,1,4]{0,2,1:T(4,128)S(1)}, f32[256,1,4,128]{3,0,2,1:T(8,128)S(1)}) conditional(s32[]{:T(128)} %convert_element_type.56, () %tuple.13, (s32[]{:T(128)}, s32[256]{0:T(256)S(1)}, s32[1,4096]{1,0:T(1,128)S(1)}, s32[256]{0:T(256)}, bf16[256,512]{1,0:T(8,128)(2,1)}, /*index=5*/bf16[128,4096]{0,1:T(8,128)(2,1)}, f32[256,4]{0,1:T(4,128)}, ...), branch_computations={%region_0.0_spmd, %region_1.4_spmd} | conditional | flops 2230320384 | bytes 61874252 | solution.py:104
  124.7 2.5 fusion.8
  127.3 5.5 %fusion.3 = (f32[256,4]{0,1:T(4,128)S(1)}, f32[4096,256,4]{1,0,2:T(8,128)S(1)}) fusion(f32[4,4096]{1,0:T(4,128)S(1)} %get-tuple-element.33, f32[256,4]{0,1:T(4,128)} %get-tuple-element.32, pred[256,4096]{0,1:T(8,128)(4,1)S(1)} %fusion.8, bf16[128,4096]{0,1:T(8,128)(2,1)} %get-tuple-element.30, bf16[256,512]{1,0:T(8,128)(2,1)} %get-tuple-element.40), kind=kOutput, calls=%fused_computation.7 | convolution fusion | flops 1094712320 | bytes 19210240 | tf_op jit(solution)/shard_map/cond/branch_1_fun/qagd,adk->qagk/dot_general | solution.py:82
  132.8 6.8 %fusion.9 = f32[256,1,4,128]{3,0,2,1:T(8,128)S(1)} fusion(f32[4096,256,4]{1,0,2:T(8,128)S(1)} %get-tuple-element.44, f32[256,4]{0,1:T(4,128)S(1)} %broadcast_maximum_fusion, f32[4,4096]{1,0:T(4,128)S(1)} %get-tuple-element.33, f32[256,4]{0,1:T(4,128)S(1)} %copy-done.5, pred[256,4096]{0,1:T(8,128)(4,1)S(1)} %fusion.8, bf16[128,4096]{1,0:T(8,128)(2,1)S(1)} %copy-done.9), kind=kOutput, calls=%fused_computation.13 | convolution fusion | flops 1103101952 | bytes 19472384 | tf_op jit(solution)/shard_map/cond/branch_1_fun/qagk,adk->qagd/dot_general | solution.py:95
  139.7 5.8 %fusion.2 = f32[256,4]{0,1:T(4,128)S(1)} fusion(f32[4096,256,4]{1,0,2:T(8,128)S(1)} %get-tuple-element.44, f32[256,4]{0,1:T(4,128)S(1)} %broadcast_maximum_fusion, f32[4,4096]{1,0:T(4,128)S(1)} %get-tuple-element.33, f32[256,4]{0,1:T(4,128)S(1)} %copy-done.5, pred[256,4096]{0,1:T(8,128)(4,1)S(1)} %fusion.8), kind=kLoop, calls=%fused_computation.6 | loop fusion | flops 29359104 | bytes 17903616 | tf_op jit(solution)/shard_map/cond/branch_1_fun/reduce_sum | solution.py:94
  146.0 3.9 %all_to_all.29 = bf16[2,128,512]{2,1,0:T(8,128)(2,1)S(1)} all-to-all(bf16[2,128,512]{2,1,0:T(8,128)(2,1)S(1)} %all_to_all.20), channel_id=1, replica_groups=mesh['sp'=16,'tp'=2] {'tp'}, dimensions={0} | all-to-all | bytes 524288 | tf_op jit(solution)/shard_map/all_to_all | solution.py:110
  150.1 2.9 convolution_convert_fusion.2
  154.0 1.2 convolution_convert_fusion.1
  155.2 96.7 %all_to_all.30 = bf16[32,32,2048]{2,1,0:T(8,128)(2,1)S(1)} all-to-all(bf16[32,32,2048]{2,1,0:T(8,128)(2,1)S(1)} %bitcast.161), channel_id=1, replica_groups=mesh['sp'=16,'tp'=2] {'sp','tp'}, dimensions={0} | all-to-all | bytes 8388608 | tf_op jit(solution)/shard_map/all_to_all | solution.py:132
  252.0 2.0 copy-done.3
  253.9 3.7 fusion.22
  257.7 10.1 %convolution_convert_fusion = bf16[32,32,2048]{2,1,0:T(8,128)(2,1)} fusion(bf16[1,512,2048]{2,1,0:T(8,128)(2,1)S(1)} %copy-done, f32[32,32,512]{2,1,0:T(8,128)} %fusion.22, bf16[32,32,2048]{2,1,0:T(8,128)(2,1)} %copy-done.3, bf16[1,2048,512]{2,1,0:T(8,128)(2,1)} %param.29), kind=kOutput, calls=%fused_computation.24 | convolution fusion | flops 4300210176 | bytes 14680064 | tf_op jit(solution)/shard_map/nemf,efd->nemd/dot_general | solution.py:29
  267.7 4.0 %all-to-all-start.2 = ((bf16[32,32,2048]{2,1,0:T(8,128)(2,1)}), bf16[32,32,2048]{2,1,0:T(8,128)(2,1)}, u32[]{:S(2)}, u32[]{:S(2)}) async-start(bf16[32,32,2048]{2,1,0:T(8,128)(2,1)} %convolution_convert_fusion), calls=%async_computation.2 | async-start | bytes 8388608 | tf_op jit(solution)/shard_map/all_to_all | solution.py:137
  272.4 2.0 fusion.58
  274.4 91.0 %all-to-all-done.2 = bf16[32,32,2048]{2,1,0:T(8,128)(2,1)} async-done(((bf16[32,32,2048]{2,1,0:T(8,128)(2,1)}), bf16[32,32,2048]{2,1,0:T(8,128)(2,1)}, u32[]{:S(2)}, u32[]{:S(2)}) %all-to-all-start.2) | async-done | bytes 4194336 | tf_op jit(solution)/shard_map/all_to_all | solution.py:137
  365.5 8.0 %gather_fusion = bf16[512,2048]{1,0:T(8,128)(2,1)} fusion(bf16[1024,2048]{1,0:T(8,128)(2,1)} %bitcast.35, s32[1024]{0:T(1024)S(1)} %pad_clamp_fusion), kind=kCustom, calls=%fused_computation | custom fusion | bytes 4196352 | tf_op jit(solution)/shard_map/jit(_take)/gather | solution.py:139
  373.5 4.1 %gather.7 = bf16[128,4,2048]{2,1,0:T(4,128)(2,1)} reshape(bf16[512,2048]{1,0:T(8,128)(2,1)} %gather_fusion) | data formatting | bytes 4194304 | tf_op jit(solution)/shard_map/jit(_take)/gather | solution.py:139
  377.6 3.9 fusion.29
  381.5 4.0 %fusion.57 = (f32[128]{0:T(128)S(1)}, f32[128,2048]{1,0:T(8,128)S(1)}) fusion(bf16[512,2048]{1,0:T(8,128)(2,1)} %param.34, bf16[128,2048]{1,0:T(8,128)(2,1)} %copy-done.1, bf16[2048,512]{1,0:T(8,128)(2,1)} %param.33, f32[128,512]{1,0:T(8,128)S(1)} %fusion.58, f32[128,1,2048]{2,1,0:T(1,128)} %fusion.29), kind=kOutput, calls=%fused_computation.85 | convolution fusion | flops 538574720 | bytes 7078400 | tf_op jit(solution)/shard_map/dot_general | solution.py:144
  (64 shorter events, 9.3 us)
Async XLA Ops:
  6.5 251.1 %copy-start = (bf16[1,512,2048]{2,1,0:T(8,128)(2,1)S(1)}, bf16[1,512,2048]{2,1,0:T(8,128)(2,1)}, u32[]{:S(2)}) copy-start(bf16[1,512,2048]{2,1,0:T(8,128)(2,1)} %param.31) | copy-start | bytes 6291460
  6.5 88.9 %all-gather.5.cloned.1.call-start = ((), (), s32[]{:S(2)}) async-start(), calls=%async_computation.3 | async-start | bytes 1114112 | tf_op jit(solution)/shard_map/all_gather | solution.py:72
  8.3 116.4 %all-gather.7.cloned.1.call-start = ((), (), s32[]{:S(2)}) async-start(), calls=%async_computation.4 | async-start | bytes 1114112 | tf_op jit(solution)/shard_map/all_gather | solution.py:73
  127.3 5.5 %copy-start.5 = (f32[256,4]{0,1:T(4,128)S(1)}, f32[256,4]{0,1:T(4,128)}, u32[]{:S(2)}) copy-start(f32[256,4]{0,1:T(4,128)} %get-tuple-element.32) | copy-start | bytes 12292 | tf_op jit(solution)/shard_map/cond
  127.3 5.5 %copy-start.9 = (bf16[128,4096]{1,0:T(8,128)(2,1)S(1)}, bf16[128,4096]{1,0:T(8,128)(2,1)}, u32[]{:S(2)}) copy-start(bf16[128,4096]{1,0:T(8,128)(2,1)} %get-tuple-element.34) | copy-start | bytes 3145732 | tf_op jit(solution)/shard_map/cond
  145.5 7.6 %copy-start.2 = (bf16[128,2048]{1,0:T(8,128)(2,1)S(1)}, bf16[128,2048]{1,0:T(8,128)(2,1)}, u32[]{:S(2)}) copy-start(bf16[128,2048]{1,0:T(8,128)(2,1)} %param.24) | copy-start | bytes 1572868
  154.0 118.4 %copy-start.1 = (bf16[128,2048]{1,0:T(8,128)(2,1)}, bf16[128,2048]{1,0:T(8,128)(2,1)S(1)}, u32[]{:S(2)}) copy-start(bf16[128,2048]{1,0:T(8,128)(2,1)S(1)} %multiply_convert_fusion.1) | copy-start | bytes 1572868
  155.2 98.7 %copy-start.8 = (bf16[1,2048,512]{2,1,0:T(8,128)(2,1)S(1)}, bf16[1,2048,512]{2,1,0:T(8,128)(2,1)}, u32[]{:S(2)}) copy-start(bf16[1,2048,512]{2,1,0:T(8,128)(2,1)} %param.30) | copy-start | bytes 6291460
  252.0 2.0 copy-start.3
  267.7 4.0 %copy-start.4 = (s32[128,4]{0,1:T(4,128)S(1)}, s32[128,4]{0,1:T(4,128)}, u32[]{:S(2)}) copy-start(s32[128,4]{0,1:T(4,128)} %param.27) | copy-start | bytes 6148
  267.7 4.4 %copy-start.7 = (f32[128,4]{0,1:T(4,128)S(1)}, f32[128,4]{0,1:T(4,128)}, u32[]{:S(2)}) copy-start(f32[128,4]{0,1:T(4,128)} %param.28) | copy-start | bytes 6148
  267.7 4.6 %copy-start.6 = (bf16[2048]{0:T(1024)(128)(2,1)S(1)}, bf16[2048]{0:T(1024)(128)(2,1)}, u32[]{:S(2)}) copy-start(bf16[2048]{0:T(1024)(128)(2,1)} %param.35) | copy-start | bytes 12292
  267.7 97.7 %all-to-all-start.2 = ((bf16[32,32,2048]{2,1,0:T(8,128)(2,1)}), bf16[32,32,2048]{2,1,0:T(8,128)(2,1)}, u32[]{:S(2)}, u32[]{:S(2)}) async-start(bf16[32,32,2048]{2,1,0:T(8,128)(2,1)} %convolution_convert_fusion), calls=%async_computation.2 | async-start | bytes 8388608 | tf_op jit(solution)/shard_map/all_to_all | solution.py:137
Sparse Core Ops, SparseCore 0:
  10.1 57.9 all-gather.4
  70.8 53.9 all-gather.6
where the time goes:
time: 394 us
  blocking collectives  180 us (46%)
  waiting for transfers between devices  121 us (31%)
  matrix products  40.2 us (10%)
  local copies, waits for them, and re-layouts  20.1 us (5%)
  between operations  14.9 us (4%)
  other arithmetic  13.8 us (4%)
  starting transfers between devices  4.06 us (1%)
    all_to_all x1, blocking collectives, local(): lax.all_to_all(outgoing, ('sp', 'tp'), split_axis=0, concat_axis=0, tiled...  96.7 us
    all_to_all x1, waiting for transfers between devices, local(): lax.all_to_all(finished, ('sp', 'tp'), split_axis=0, concat_axis=0, tiled...  91 us
    all_gather x1, blocking collectives, local(): lax.all_gather(documents.reshape(1, tok_rows), 'sp', axis=1, tiled=True)  42.7 us
    all_gather x1, blocking collectives, local(): lax.all_gather(gate_cache, 'sp', axis=1, tiled=True)  36.1 us
    all_gather x1, waiting for transfers between devices, local(): value_piece = lax.all_gather(values, 'sp', axis=1, tiled=True)  29.3 us
    gather x2, local copies, waits for them, and re-layouts, local(): jnp.take(returned, slots, axis=0).reshape(row_count, top_count, width_model)  12.1 us
    dot_general x1, matrix products, expert_block(): jnp.einsum('nemf,efd->nemd', hidden, expert_down, preferred_element_type=...  10.1 us
  transfers between devices with their start and end apart: 3, of which 2 were waited for; matrix products, arithmetic and copies ran while one was open for 2% of the time, Pallas kernels for 0%

commit v1 on v0

--- a/solution.py
+++ b/solution.py
@@ -49,6 +49,14 @@
     shared_down,
     ffn_gain,
 ):
+
+    def scan_bands(frame_in, block_in):
+        return jnp.split(
+            lax.all_gather(jnp.concatenate([frame_in, block_in], axis=0), "sp", tiled=True, axis=1),
+            [frame_in.shape[0]],
+            axis=0,
+        )
+
     tok_rows = queries.shape[0]
     local_heads = gate_cache.shape[0]
     kv_local = keys.shape[0] // HD
@@ -69,8 +77,7 @@
         jnp.zeros((tok_rows, kv_local, group_size), jnp.float32),
         jnp.zeros((tok_rows, kv_local, group_size, HD), jnp.float32),
     )
-    key_piece = lax.all_gather(keys, "sp", axis=1, tiled=True)
-    value_piece = lax.all_gather(values, "sp", axis=1, tiled=True)
+    key_piece, value_piece = scan_bands(keys, values)
     width_keys = key_piece.shape[1]
     key_cum = all_cache.reshape(kv_local, group_size, width_keys)
 

time: 394 us -> 379 us (0.962)
  waiting for transfers between devices: 121 us -> 91.1 us
  matrix products: 40.2 us -> 49.2 us
  local copies, waits for them, and re-layouts: 20.1 us -> 24.5 us
    all_gather x2 -> x1, waiting for transfers between devices: 29.3 us -> 0.02 us  [scan_bands(): lax.all_gather(jnp.concatenate([frame_in, block_in], axis=0), 'sp', tiled...]
    dot_general x1, matrix products: 6.82 us -> 11.6 us  [update(): jnp.einsum('qagk,adk->qagd', weights.astype(jnp.bfloat16), value_block, p...]
    dot_general x1, matrix products: 5.47 us -> 9.79 us  [update(): jnp.einsum('qagd,adk->qagk', grouped_q, key_block, preferred_element_type...]
    another operation x1 -> x2, local copies, waits for them, and re-layouts: 0.01 us -> 4.13 us
  transfers between devices with their start and end apart: 3 -> 2, of which waited for: 2 -> 1; matrix products, arithmetic and copies ran while one was open for 2% -> 2% of each run, Pallas kernels for 0% -> 0%
where the time goes in v1:
time: 379 us; the launch traced here: 378 us
  blocking collectives  179 us (47%)
  waiting for transfers between devices  91.1 us (24%)
  matrix products  49.2 us (13%)
  local copies, waits for them, and re-layouts  24.5 us (6%)
  other arithmetic  15.7 us (4%)
  between operations  14.9 us (4%)
  starting transfers between devices  3.8 us (1%)
    all_to_all x1, blocking collectives, local(): lax.all_to_all(outgoing, ('sp', 'tp'), split_axis=0, concat_axis=0, tiled...  95.6 us
    all_to_all x1, waiting for transfers between devices, local(): lax.all_to_all(finished, ('sp', 'tp'), split_axis=0, concat_axis=0, tiled...  91 us
    all_gather x1, blocking collectives, local(): lax.all_gather(documents.reshape(1, tok_rows), 'sp', axis=1, tiled=True)  42.8 us
    all_gather x1, blocking collectives, local(): lax.all_gather(gate_cache, 'sp', axis=1, tiled=True)  36.5 us
    gather x2, local copies, waits for them, and re-layouts, local(): jnp.take(returned, slots, axis=0).reshape(row_count, top_count, width_model)  12.1 us
    dot_general x1, matrix products, update(): jnp.einsum('qagk,adk->qagd', weights.astype(jnp.bfloat16), value_block, p...  11.6 us
    dot_general x1, matrix products, expert_block(): jnp.einsum('nemf,efd->nemd', hidden, expert_down, preferred_element_type=...  10 us
    dot_general x1, matrix products, update(): jnp.einsum('qagd,adk->qagk', grouped_q, key_block, preferred_element_type...  9.79 us
  transfers between devices with their start and end apart: 2, of which 1 were waited for; matrix products, arithmetic and copies ran while one was open for 2% of the time, Pallas kernels for 0%

profile of v1, /device:TPU:0, one launch (start us, length us, event | category | flops | bytes accessed | tf_op | source)
XLA Modules:
  0.0 378.1 jit_solution(15300692476622716140)
XLA Ops:
  10.3 1.2 slice.14
  11.5 42.8 %all-gather.1 = s32[16,1,256]{2,1,0:T(1,128)S(1)} all-gather(s32[1,1,256]{2,1,0:T(1,128)} %bitcast.172), channel_id=2, replica_groups=mesh['sp'=16,'tp'=2] {'sp'}, dimensions={0}, use_global_device_ids=true | all-gather | bytes 17408 | tf_op jit(solution)/shard_map/all_gather | solution.py:72
  58.6 36.5 %all_gather.11 = f32[4,4096]{1,0:T(4,128)S(1)} all-gather(f32[4,256]{1,0:T(4,128)} %param.22), channel_id=1, replica_groups=mesh['sp'=16,'tp'=2] {'sp'}, dimensions={1}, use_global_device_ids=true | all-gather | bytes 69632 | tf_op jit(solution)/shard_map/all_gather | solution.py:71
  96.2 33.9 %conditional.1 = (f32[256,1,4]{0,2,1:T(4,128)S(1)}, f32[256,1,4,128]{3,0,2,1:T(8,128)}) conditional(s32[]{:T(128)} %convert_element_type.56, () %tuple.13, (s32[]{:T(128)}, s32[256]{0:T(256)S(1)}, s32[1,4096]{1,0:T(1,128)S(1)}, s32[256]{0:T(256)}, bf16[256,4096]{0,1:T(8,128)(2,1)}, /*index=5*/bf16[256,512]{1,0:T(8,128)(2,1)}, f32[256,4]{0,1:T(4,128)}, ...), branch_computations={%region_0.0_spmd, %region_1.4_spmd} | conditional | flops 2230320384 | bytes 128983112 | solution.py:111
  96.2 2.6 fusion.8
  98.8 9.8 %fusion.3 = (f32[256,4]{0,1:T(4,128)S(1)}, f32[4096,256,4]{1,0,2:T(8,128)}) fusion(f32[4,4096]{1,0:T(4,128)S(1)} %get-tuple-element.34, f32[256,4]{0,1:T(4,128)} %get-tuple-element.33, pred[256,4096]{0,1:T(8,128)(4,1)S(1)} %fusion.8, bf16[256,4096]{0,1:T(8,128)(2,1)} %get-tuple-element.31, bf16[256,512]{1,0:T(8,128)(2,1)} %get-tuple-element.40), kind=kOutput, calls=%fused_computation.7 | convolution fusion | flops 1094712320 | bytes 19210240 | tf_op jit(solution)/shard_map/cond/branch_1_fun/qagd,adk->qagk/dot_general | solution.py:89
  108.6 4.1 %copy.63 = bf16[256,4096]{1,0:T(8,128)(2,1)} copy(bf16[256,4096]{0,1:T(8,128)(2,1)} %get-tuple-element.31) | data formatting | bytes 4194304 | tf_op jit(solution)/shard_map
  112.7 11.6 %fusion.9 = f32[256,1,4,128]{3,0,2,1:T(8,128)} fusion(f32[4096,256,4]{1,0,2:T(8,128)} %get-tuple-element.44, f32[256,4]{0,1:T(4,128)S(1)} %broadcast_maximum_fusion, f32[4,4096]{1,0:T(4,128)S(1)} %get-tuple-element.34, f32[256,4]{0,1:T(4,128)S(1)} %copy-done.6, pred[256,4096]{0,1:T(8,128)(4,1)S(1)} %fusion.8, bf16[256,4096]{1,0:T(8,128)(2,1)} %copy.63), kind=kOutput, calls=%fused_computation.13 | convolution fusion | flops 1103101952 | bytes 19472384 | tf_op jit(solution)/shard_map/cond/branch_1_fun/qagk,adk->qagd/dot_general | solution.py:102
  124.3 5.8 %fusion.2 = f32[256,4]{0,1:T(4,128)S(1)} fusion(f32[4096,256,4]{1,0,2:T(8,128)S(1)} %copy-done.1, f32[256,4]{0,1:T(4,128)S(1)} %broadcast_maximum_fusion, f32[4,4096]{1,0:T(4,128)S(1)} %get-tuple-element.34, f32[256,4]{0,1:T(4,128)S(1)} %copy-done.6, pred[256,4096]{0,1:T(8,128)(4,1)S(1)} %fusion.8), kind=kLoop, calls=%fused_computation.6 | loop fusion | flops 29359104 | bytes 17903616 | tf_op jit(solution)/shard_map/cond/branch_1_fun/reduce_sum | solution.py:101
  130.1 1.3 divide_convert_fusion
  131.8 3.9 %all_to_all.29 = bf16[2,128,512]{2,1,0:T(8,128)(2,1)S(1)} all-to-all(bf16[2,128,512]{2,1,0:T(8,128)(2,1)S(1)} %all_to_all.20), channel_id=1, replica_groups=mesh['sp'=16,'tp'=2] {'tp'}, dimensions={0} | all-to-all | bytes 524288 | tf_op jit(solution)/shard_map/all_to_all | solution.py:117
  135.9 2.9 convolution_convert_fusion.2
  139.8 1.2 convolution_convert_fusion.1
  141.0 95.6 %all_to_all.30 = bf16[32,32,2048]{2,1,0:T(8,128)(2,1)S(1)} all-to-all(bf16[32,32,2048]{2,1,0:T(8,128)(2,1)S(1)} %bitcast.161), channel_id=1, replica_groups=mesh['sp'=16,'tp'=2] {'sp','tp'}, dimensions={0} | all-to-all | bytes 8388608 | tf_op jit(solution)/shard_map/all_to_all | solution.py:139
  236.6 2.0 copy-done.4
  238.6 3.7 fusion.22
  242.3 10.0 %convolution_convert_fusion = bf16[32,32,2048]{2,1,0:T(8,128)(2,1)} fusion(bf16[1,512,2048]{2,1,0:T(8,128)(2,1)S(1)} %copy-done, f32[32,32,512]{2,1,0:T(8,128)} %fusion.22, bf16[32,32,2048]{2,1,0:T(8,128)(2,1)} %copy-done.4, bf16[1,2048,512]{2,1,0:T(8,128)(2,1)} %param.29), kind=kOutput, calls=%fused_computation.25 | convolution fusion | flops 4300210176 | bytes 14680064 | tf_op jit(solution)/shard_map/nemf,efd->nemd/dot_general | solution.py:29
  252.4 3.8 %all-to-all-start.2 = ((bf16[32,32,2048]{2,1,0:T(8,128)(2,1)}), bf16[32,32,2048]{2,1,0:T(8,128)(2,1)}, u32[]{:S(2)}, u32[]{:S(2)}) async-start(bf16[32,32,2048]{2,1,0:T(8,128)(2,1)} %convolution_convert_fusion), calls=%async_computation.2 | async-start | bytes 8388608 | tf_op jit(solution)/shard_map/all_to_all | solution.py:144
  256.8 2.0 fusion.58
  258.8 91.0 %all-to-all-done.2 = bf16[32,32,2048]{2,1,0:T(8,128)(2,1)} async-done(((bf16[32,32,2048]{2,1,0:T(8,128)(2,1)}), bf16[32,32,2048]{2,1,0:T(8,128)(2,1)}, u32[]{:S(2)}, u32[]{:S(2)}) %all-to-all-start.2) | async-done | bytes 4194336 | tf_op jit(solution)/shard_map/all_to_all | solution.py:144
  349.9 8.0 %gather_fusion = bf16[512,2048]{1,0:T(8,128)(2,1)} fusion(bf16[1024,2048]{1,0:T(8,128)(2,1)} %bitcast.35, s32[1024]{0:T(1024)S(1)} %pad_clamp_fusion), kind=kCustom, calls=%fused_computation | custom fusion | bytes 4196352 | tf_op jit(solution)/shard_map/jit(_take)/gather | solution.py:146
  357.9 4.1 %gather.7 = bf16[128,4,2048]{2,1,0:T(4,128)(2,1)} reshape(bf16[512,2048]{1,0:T(8,128)(2,1)} %gather_fusion) | data formatting | bytes 4194304 | tf_op jit(solution)/shard_map/jit(_take)/gather | solution.py:146
  362.0 3.9 %fusion.29 = f32[128,1,2048]{2,1,0:T(1,128)} fusion(bf16[128,4,1]{1,2,0:T(2,128)(2,1)S(1)} %copy.76, bf16[128,4,2048]{2,1,0:T(4,128)(2,1)} %gather.7, pred[128,4]{1,0:T(8,128)(4,1)S(1)} %copy.73), kind=kOutput, calls=%fused_computation.42 | convolution fusion | flops 3145728 | bytes 3147264 | tf_op jit(solution)/shard_map/rkd,rk->rd/dot_general | solution.py:147
  365.9 4.0 %fusion.57 = (f32[128]{0:T(128)S(1)}, f32[128,2048]{1,0:T(8,128)S(1)}) fusion(bf16[512,2048]{1,0:T(8,128)(2,1)} %param.34, bf16[128,2048]{1,0:T(8,128)(2,1)} %copy-done.2, bf16[2048,512]{1,0:T(8,128)(2,1)} %param.33, f32[128,512]{1,0:T(8,128)S(1)} %fusion.58, f32[128,1,2048]{2,1,0:T(1,128)} %fusion.29), kind=kOutput, calls=%fused_computation.87 | convolution fusion | flops 538574720 | bytes 7078400 | tf_op jit(solution)/shard_map/dot_general | solution.py:151
  (64 shorter events, 11.1 us)
Async XLA Ops:
  6.5 235.8 %copy-start = (bf16[1,512,2048]{2,1,0:T(8,128)(2,1)S(1)}, bf16[1,512,2048]{2,1,0:T(8,128)(2,1)}, u32[]{:S(2)}) copy-start(bf16[1,512,2048]{2,1,0:T(8,128)(2,1)} %param.31) | copy-start | bytes 6291460
  6.5 89.6 %all-gather.4.cloned.1.call-start = ((), (), s32[]{:S(2)}) async-start(), calls=%async_computation.3 | async-start | bytes 2228224 | tf_op jit(solution)/shard_map/all_gather | solution.py:55
  108.6 4.1 %copy-start.6 = (f32[256,4]{0,1:T(4,128)S(1)}, f32[256,4]{0,1:T(4,128)}, u32[]{:S(2)}) copy-start(f32[256,4]{0,1:T(4,128)} %get-tuple-element.33) | copy-start | bytes 12292 | tf_op jit(solution)/shard_map/cond
  112.7 11.6 %copy-start.1 = (f32[4096,256,4]{1,0,2:T(8,128)S(1)}, f32[4096,256,4]{1,0,2:T(8,128)}, u32[]{:S(2)}) copy-start(f32[4096,256,4]{1,0,2:T(8,128)} %get-tuple-element.44) | copy-start | bytes 50331652 | tf_op jit(solution)/shard_map/cond
  130.1 8.7 %copy-start.3 = (bf16[128,2048]{1,0:T(8,128)(2,1)S(1)}, bf16[128,2048]{1,0:T(8,128)(2,1)}, u32[]{:S(2)}) copy-start(bf16[128,2048]{1,0:T(8,128)(2,1)} %param.24) | copy-start | bytes 1572868
  139.7 117.0 %copy-start.2 = (bf16[128,2048]{1,0:T(8,128)(2,1)}, bf16[128,2048]{1,0:T(8,128)(2,1)S(1)}, u32[]{:S(2)}) copy-start(bf16[128,2048]{1,0:T(8,128)(2,1)S(1)} %multiply_convert_fusion.1) | copy-start | bytes 1572868
  141.0 97.6 %copy-start.9 = (bf16[1,2048,512]{2,1,0:T(8,128)(2,1)S(1)}, bf16[1,2048,512]{2,1,0:T(8,128)(2,1)}, u32[]{:S(2)}) copy-start(bf16[1,2048,512]{2,1,0:T(8,128)(2,1)} %param.30) | copy-start | bytes 6291460
  236.6 2.0 copy-start.4
  252.4 3.8 %copy-start.5 = (s32[128,4]{0,1:T(4,128)S(1)}, s32[128,4]{0,1:T(4,128)}, u32[]{:S(2)}) copy-start(s32[128,4]{0,1:T(4,128)} %param.27) | copy-start | bytes 6148
  252.4 4.2 %copy-start.8 = (f32[128,4]{0,1:T(4,128)S(1)}, f32[128,4]{0,1:T(4,128)}, u32[]{:S(2)}) copy-start(f32[128,4]{0,1:T(4,128)} %param.28) | copy-start | bytes 6148
  252.4 4.4 %copy-start.7 = (bf16[2048]{0:T(1024)(128)(2,1)S(1)}, bf16[2048]{0:T(1024)(128)(2,1)}, u32[]{:S(2)}) copy-start(bf16[2048]{0:T(1024)(128)(2,1)} %param.35) | copy-start | bytes 12292
  252.4 97.5 %all-to-all-start.2 = ((bf16[32,32,2048]{2,1,0:T(8,128)(2,1)}), bf16[32,32,2048]{2,1,0:T(8,128)(2,1)}, u32[]{:S(2)}, u32[]{:S(2)}) async-start(bf16[32,32,2048]{2,1,0:T(8,128)(2,1)} %convolution_convert_fusion), calls=%async_computation.2 | async-start | bytes 8388608 | tf_op jit(solution)/shard_map/all_to_all | solution.py:144
Sparse Core Ops, SparseCore 0:
  10.1 63.3 all-gather.3
